TPU v7x, 32 devices: a whole 2x2x4 slice. The times are simulated.
32 devices in a mesh: sp: 16 (over z, y, x), tp: 2 (over core).
Axes of the slice: x: 2, y: 2, z: 4, core: 2. Of those that a mesh axis runs over, the one named last changes fastest.
Arguments:
- queries_small: bfloat16 [4096, 1024], P('sp', 'tp'), may hold values from -160 to 160
- queries_large: bfloat16 [4096, 1024], P('sp', 'tp'), may hold values from -160 to 160
- kv_small: bfloat16 [4096, 128], P('sp'), may hold values from -4 to 4
- kv_large: bfloat16 [4096, 256], P('sp'), may hold values from -4 to 4
- cum_small: float32 [16, 4096], P('tp', 'sp'), may hold values from -514 to 0, as said below
- cum_large: float32 [8, 4096], P('tp', 'sp'), may hold values from -514 to 0, as said below
- residual: bfloat16 [4096, 2048], P(('sp', 'tp')), may hold values from -6 to 6
- out_small: bfloat16 [1024, 2048], replicated, may hold values from -0.125 to 0.125
- out_large: bfloat16 [1024, 2048], replicated, may hold values from -0.125 to 0.125
- gain_mix: float32 [2048], replicated, may hold values from 0.1 to 1.9
- gain_route: float32 [2048], replicated, may hold values from 0.1 to 1.9
- gain_blend: float32 [2048], replicated, may hold values from 0.1 to 1.9
- w_gate: bfloat16 [32, 2048, 1024], P(('sp', 'tp')), may hold values from -0.125 to 0.125
- w_up: bfloat16 [32, 2048, 1024], P(('sp', 'tp')), may hold values from -0.125 to 0.125
- w_down: bfloat16 [32, 1024, 2048], P(('sp', 'tp')), may hold values from -0.1875 to 0.1875
- route: int32 [2, 4096], P(None, ('sp', 'tp')), may hold values from 0 to 31, as said below
- route_bias: float32 [4096], P(('sp', 'tp')), may hold values from -6 to 6
Outputs:
- result: bfloat16 [4096, 2048], P(('sp', 'tp'))
Inputs may be any that keep to these rules, and one draw needn't show every extreme that they name: `cum_small`: each row is non-increasing along positions. `cum_large`: each row is non-increasing along positions. route[0, t] and route[1, t] are different experts of the same group of 8 consecutive experts. Among the 128 positions of one device (aligned blocks), no expert is named by more than 16 of them; in every draw all experts of one group are named by exactly 16 positions of every device. Within one device's positions the loads of the experts of one group differ by at most 2.
All inputs are finite; a program needn't handle non-finite values.
Results may differ from a plain program's by a relative error of at most 0.014.
Values may be sent and summed in bfloat16 or wider, within the bound.
A program may use at most 128 MiB of HBM per device.

v0:
```python
import math

import jax
import jax.numpy as jnp
from jax import lax
from jax.sharding import PartitionSpec as P

norm_eps = 1e-06
far_score = -1e30


def rms_scale(values, gain_row):
    return (
        values * lax.rsqrt(jnp.mean(values * values, axis=-1, keepdims=True) + norm_eps) * gain_row
    )


def online_update(carried, queries, query_cum, keys_values, key_cum, key_pos, query_pos):
    running_max, running_sum, weighted = carried
    head_size = keys_values.shape[1] // 2
    key_rows = keys_values[:, :head_size]
    value_rows = keys_values[:, head_size:]
    scores = jnp.einsum(
        "qhd,kd->hqk", queries, key_rows, preferred_element_type=jnp.float32
    ) * head_size ** (-0.5)
    scores = scores + query_cum[:, :, None] - key_cum[:, None, :]
    allowed = key_pos[None, None, :] <= query_pos[None, :, None]
    scores = jnp.where(allowed, scores, far_score)
    newest = jnp.maximum(running_max, jnp.max(scores, axis=-1))
    weights = jnp.where(allowed, jnp.exp(scores - newest[:, :, None]), 0.0)
    factor = jnp.exp(running_max - newest)
    running_sum = running_sum * factor + jnp.sum(weights, axis=-1)
    weighted = weighted * factor[:, :, None] + jnp.einsum(
        "hqk,kd->hqd", weights.astype(jnp.bfloat16), value_rows, preferred_element_type=jnp.float32
    )
    return (newest, running_sum, weighted)


def attend_keys(
    softmax_state,
    query_small,
    query_large,
    qcum_small,
    qcum_large,
    query_pos,
    part_small,
    part_large,
    key_pos,
    kcum_small,
    kcum_large,
):
    key_count = key_pos.shape[0]
    block_width = math.gcd(key_count, 2048)
    blocks = key_count // block_width
    pieces = (
        part_small.reshape(blocks, block_width, part_small.shape[1]),
        part_large.reshape(blocks, block_width, part_large.shape[1]),
        key_pos.reshape(blocks, block_width),
        kcum_small.reshape(kcum_small.shape[0], blocks, block_width).transpose(1, 0, 2),
        kcum_large.reshape(kcum_large.shape[0], blocks, block_width).transpose(1, 0, 2),
    )
    query_last = query_pos[-1]

    def advance(carried, block_data):
        kv_one, kv_two, positions, cum_one, cum_two = block_data

        def compute(current):
            return (
                online_update(
                    current[0], query_small, qcum_small, kv_one, cum_one, positions, query_pos
                ),
                online_update(
                    current[1], query_large, qcum_large, kv_two, cum_two, positions, query_pos
                ),
            )

        return (
            lax.cond(jnp.min(positions) <= query_last, compute, lambda current: current, carried),
            None,
        )

    softmax_state, _ = lax.scan(advance, softmax_state, pieces)
    return softmax_state


def finish(carried):
    running_max, running_sum, weighted = carried
    outputs = (weighted / running_sum[:, :, None]).astype(jnp.bfloat16)
    return outputs.transpose(1, 0, 2).reshape(outputs.shape[1], outputs.shape[0] * outputs.shape[2])


def fresh_state(head_count, query_count, head_size):
    return (
        jnp.full((head_count, query_count), far_score, jnp.float32),
        jnp.zeros((head_count, query_count), jnp.float32),
        jnp.zeros((head_count, query_count, head_size), jnp.float32),
    )


def on_device(
    queries_small,
    queries_large,
    kv_small,
    kv_large,
    cum_small,
    cum_large,
    residual,
    out_small,
    out_large,
    gain_mix,
    gain_route,
    gain_blend,
    w_gate,
    w_up,
    w_down,
    route,
    route_bias,
):
    tokens_here = queries_small.shape[0]
    heads_small = cum_small.shape[0]
    heads_large = cum_large.shape[0]
    size_small = kv_small.shape[1] // 2
    size_large = kv_large.shape[1] // 2
    query_small = queries_small.reshape(tokens_here, heads_small, size_small)
    query_large = queries_large.reshape(tokens_here, heads_large, size_large)
    query_pos = lax.axis_index("sp") * tokens_here + jnp.arange(tokens_here, dtype=jnp.int32)
    cum_all = (
        lax.all_gather(cum_small, "sp", axis=1, tiled=True),
        lax.all_gather(cum_large, "sp", axis=1, tiled=True),
    )
    start_state = (
        fresh_state(heads_small, tokens_here, size_small),
        fresh_state(heads_large, tokens_here, size_large),
    )
    block_data = (
        lax.all_gather(kv_small, "sp", axis=0, tiled=True),
        lax.all_gather(kv_large, "sp", axis=0, tiled=True),
    )
    key_count = block_data[0].shape[0]
    key_pos = jnp.arange(key_count, dtype=jnp.int32)
    kcum_small = cum_all[0]
    kcum_large = cum_all[1]
    softmax_state = attend_keys(
        start_state,
        query_small,
        query_large,
        cum_small,
        cum_large,
        query_pos,
        block_data[0],
        block_data[1],
        key_pos,
        kcum_small,
        kcum_large,
    )
    attn_small = finish(softmax_state[0])
    attn_large = finish(softmax_state[1])
    row_count = tokens_here // lax.axis_size("tp")
    whole_small, whole_large = (
        lax.all_to_all(attn_small, "tp", split_axis=0, concat_axis=1, tiled=True),
        lax.all_to_all(attn_large, "tp", split_axis=0, concat_axis=1, tiled=True),
    )
    mixer_out = jnp.dot(whole_small, out_small, preferred_element_type=jnp.float32) + jnp.dot(
        whole_large, out_large, preferred_element_type=jnp.float32
    )
    mixed = (residual.astype(jnp.float32) + rms_scale(mixer_out, gain_mix)).astype(jnp.bfloat16)
    routed = rms_scale(mixed.astype(jnp.float32), gain_route).astype(jnp.bfloat16)
    experts = lax.axis_size(("sp", "tp"))
    capacity = 4 * row_count // experts
    flat_ids = route.reshape(2 * row_count)
    marked = (flat_ids[:, None] == jnp.arange(experts, dtype=jnp.int32)[None, :]).astype(jnp.int32)
    ranked = jnp.sum((jnp.cumsum(marked, axis=0) - 1) * marked, axis=1)
    slot_ids = flat_ids * capacity + ranked
    dispatch_table = (
        slot_ids[:, None] == jnp.arange(experts * capacity, dtype=jnp.int32)[None, :]
    ).astype(jnp.bfloat16)
    dispatch_table = dispatch_table[:row_count] + dispatch_table[row_count:]
    outgoing = jnp.einsum(
        "rs,rd->sd", dispatch_table, routed, preferred_element_type=jnp.float32
    ).astype(jnp.bfloat16)
    outgoing = outgoing.reshape(experts, capacity, routed.shape[1])
    received = lax.all_to_all(outgoing, ("sp", "tp"), split_axis=0, concat_axis=0, tiled=True)
    row_total = received.shape[0] * received.shape[1]
    expert_rows = received.reshape(row_total, received.shape[2])
    gate_pre = jnp.dot(expert_rows, w_gate[0], preferred_element_type=jnp.float32)
    up_pre = jnp.dot(expert_rows, w_up[0], preferred_element_type=jnp.float32)
    hidden = (jax.nn.silu(gate_pre) * up_pre).astype(jnp.bfloat16)
    expert_out = jnp.dot(hidden, w_down[0], preferred_element_type=jnp.float32).astype(jnp.bfloat16)
    returned = lax.all_to_all(
        expert_out.reshape(received.shape), ("sp", "tp"), split_axis=0, concat_axis=0, tiled=True
    )
    picked = returned.reshape(experts * capacity, routed.shape[1])[slot_ids].astype(jnp.float32)
    blended = (
        jax.nn.sigmoid(route_bias)[:, None] * picked[:row_count]
        + jax.nn.sigmoid(-route_bias)[:, None] * picked[row_count:]
    )
    return (mixed.astype(jnp.float32) + rms_scale(blended, gain_blend)).astype(jnp.bfloat16)


def solution(mesh):
    in_specs = (
        P("sp", "tp"),
        P("sp", "tp"),
        P("sp", None),
        P("sp", None),
        P("tp", "sp"),
        P("tp", "sp"),
        P(("sp", "tp"), None),
        P(),
        P(),
        P(),
        P(),
        P(),
        P(("sp", "tp"), None, None),
        P(("sp", "tp"), None, None),
        P(("sp", "tp"), None, None),
        P(None, ("sp", "tp")),
        P(("sp", "tp")),
    )
    out_specs = P(("sp", "tp"), None)
    return jax.shard_map(
        on_device, mesh=mesh, in_specs=in_specs, out_specs=out_specs, check_vma=False
    )
```

profile of v0, /device:TPU:9, one launch (start us, length us, event | category | flops | bytes accessed | tf_op | source)
XLA Modules:
  0.0 332.5 jit_solution(12341823653482546608)
XLA Ops:
  8.7 1.1 copy.42
  9.8 1.1 copy.43
  12.5 28.0 %all_gather.15 = f32[4,4096]{1,0:T(4,128)S(1)} all-gather(f32[4,256]{1,0:T(4,128)} %param.26), channel_id=1, replica_groups=mesh['sp'=16,'tp'=2] {'sp'}, dimensions={1}, use_global_device_ids=true | all-gather | bytes 69632 | tf_op jit(solution)/shard_map/all_gather | solution.py:129
  40.5 30.7 %all_gather.13 = f32[8,4096]{1,0:T(8,128)S(1)} all-gather(f32[8,256]{1,0:T(8,128)} %param.25), channel_id=1, replica_groups=mesh['sp'=16,'tp'=2] {'sp'}, dimensions={1}, use_global_device_ids=true | all-gather | bytes 139264 | tf_op jit(solution)/shard_map/all_gather | solution.py:128
  71.2 0.8 fusion.58
  72.7 0.8 fusion.53
  73.5 1.5 copy.44
  75.0 52.7 %all-gather.5.cloned.1.call-done = bf16[4096,256]{1,0:T(8,128)(2,1)} async-done(((bf16[256,256]{1,0:T(8,128)(2,1)}), bf16[4096,256]{1,0:T(8,128)(2,1)}) %all-gather.5.cloned.1.call-update) | async-done | bytes 2097168 | tf_op jit(solution)/shard_map/all_gather | solution.py:137
  127.8 30.6 %while.21 = (s32[]{:T(128)}, f32[8,256]{1,0:T(8,128)S(1)}, f32[8,256]{1,0:T(8,128)S(1)}, f32[8,256,64]{1,2,0:T(8,128)S(1)}, f32[4,256]{1,0:T(4,128)S(1)}, /*inde...) while((s32[]{:T(128)}, f32[8,256]{1,0:T(8,128)S(1)}, ...), condition=%wide.region_8.9_spmd.clone, body=%wide.region_0.8_spmd.clone.sunk | while | flops 2268078336 | bytes 95699496 | solution.py:82
  127.9 0.7 fusion.72
  129.9 26.2 %conditional.3 = ((f32[8,256]{1,0:T(8,128)S(1)}, f32[8,256]{1,0:T(8,128)S(1)}, f32[8,256,64]{1,2,0:T(8,128)S(1)}, f32[4,256]{1,0:T(4,128)S(1)}, f32[4,256]{1,0:T(4,128)S(1)}, /*index=5*/f32[4,256,128]{2,1,0:T(8,128)S(1)})) conditional(s32[]{:T(128)} %convert_element_type.110, (f32[8,256]{1,0:T(8,128)S(1)}, f32[8,256]{1,0:T(8,128)S(1)}, ...), branch_computations={%region_2.2_spmd, %region_3.7_spmd} | conditional | flops 2268076288 | bytes 95681696 | solution.py:78
  130.5 5.0 %fusion.6 = (f32[8,256]{1,0:T(8,128)S(1)}, f32[2048,256,8]{1,0,2:T(8,128)S(1)}) fusion(f32[8,2048]{1,0:T(8,128)S(1)} %dynamic-slice_bitcast_fusion.2, f32[8,256]{1,0:T(8,128)} %get-tuple-element.221, pred[256,2048]{0,1:T(8,128)(4,1)S(1)} %broadcast_compare_fusion, bf16[256,8,64]{0,2,1:T(8,128)(2,1)S(1)} %get-tuple-element.220, ...), kind=kOutput, calls=%fused_computation.8 | convolution fusion | flops 557840384 | bytes 17907712 | tf_op jit(solution)/shard_map/while/body/eval_jaxpr/cond/branch_1_fun/qhd,kd->hqk/dot_general | solution.py:23
  135.5 6.0 %fusion.5 = f32[8,256]{1,0:T(8,128)S(1)} fusion(f32[2048,256,8]{1,0,2:T(8,128)S(1)} %get-tuple-element.412, f32[8,256]{1,0:T(8,128)S(1)} %max.8, f32[8,2048]{1,0:T(8,128)S(1)} %dynamic-slice_bitcast_fusion.2, f32[8,256]{1,0:T(8,128)S(1)} %copy-done.3, pred[256,2048]{0,1:T(8,128)(4,1)S(1)} %broadcast_compare_fusion), kind=kLoop, calls=%fused_computation.7 | loop fusion | flops 29358080 | bytes 17391616 | tf_op jit(solution)/shard_map/while/body/eval_jaxpr/cond/branch_1_fun/reduce_sum | solution.py:32
  141.6 5.6 %fusion.21 = f32[8,256,64]{1,2,0:T(8,128)S(1)} fusion(f32[2048,256,8]{1,0,2:T(8,128)S(1)} %get-tuple-element.412, f32[8,256]{1,0:T(8,128)S(1)} %max.8, f32[8,2048]{1,0:T(8,128)S(1)} %dynamic-slice_bitcast_fusion.2, f32[8,256]{1,0:T(8,128)S(1)} %copy-done.3, pred[256,2048]{0,1:T(8,128)(4,1)S(1)} %broadcast_compare_fusion, ...), kind=kOutput, calls=%fused_computation.21 | convolution fusion | flops 566493184 | bytes 18702336 | tf_op jit(solution)/shard_map/while/body/eval_jaxpr/cond/branch_1_fun/hqk,kd->hqd/dot_general | solution.py:33
  147.3 2.2 fusion.14
  149.5 2.9 fusion.13
  152.4 3.7 %fusion.18 = f32[4,256,128]{2,1,0:T(8,128)S(1)} fusion(f32[2048,256,4]{1,0,2:T(8,128)S(1)} %get-tuple-element.414, f32[4,256]{1,0:T(4,128)S(1)} %max.9, f32[4,2048]{1,0:T(4,128)S(1)} %dynamic-slice_bitcast_fusion.3, f32[4,256]{1,0:T(4,128)S(1)} %copy-done.4, pred[256,2048]{0,1:T(8,128)(4,1)S(1)} %broadcast_compare_fusion, ...), kind=kOutput, calls=%fused_computation.20 | convolution fusion | flops 551813120 | bytes 10530816 | tf_op jit(solution)/shard_map/while/body/eval_jaxpr/cond/branch_1_fun/hqk,kd->hqd/dot_general | solution.py:33
  158.6 0.7 copy.46
  159.9 5.2 %all_to_all.48 = bf16[2,128,512]{2,1,0:T(8,128)(2,1)S(1)} all-to-all(bf16[2,128,512]{2,1,0:T(8,128)(2,1)S(1)} %all_to_all.38), channel_id=1, replica_groups=mesh['sp'=16,'tp'=2] {'tp'}, dimensions={0} | all-to-all | bytes 524288 | tf_op jit(solution)/shard_map/all_to_all | solution.py:161
  165.1 3.8 %all-to-all-start = ((bf16[2,128,512]{1,2,0:T(8,128)(2,1)}), bf16[2,128,512]{1,2,0:T(8,128)(2,1)S(1)}, u32[]{:S(2)}, u32[]{:S(2)}) async-start(bf16[2,128,512]{1,2,0:T(8,128)(2,1)} %copy.46), calls=%async_computation | async-start | bytes 524288 | tf_op jit(solution)/shard_map/all_to_all | solution.py:160
  169.1 1.0 all-to-all-done
  170.1 2.9 fusion.62
  173.0 3.2 multiply_reduce_fusion.1
  176.6 0.8 convolution_convert_fusion
  177.4 77.4 %all_to_all.49 = bf16[32,16,2048]{2,1,0:T(8,128)(2,1)S(1)} all-to-all(bf16[32,16,2048]{2,1,0:T(8,128)(2,1)S(1)} %bitcast.126), channel_id=1, replica_groups=mesh['sp'=16,'tp'=2] {'sp','tp'}, dimensions={0} | all-to-all | bytes 4194304 | tf_op jit(solution)/shard_map/all_to_all | solution.py:182
  254.9 3.7 %fusion.36 = f32[512,1024]{1,0:T(8,128)} fusion(bf16[512,2048]{1,0:T(8,128)(2,1)S(1)} %bitcast.128, bf16[1,2048,1024]{2,1,0:T(8,128)(2,1)S(1)} %copy-done.11), kind=kOutput, calls=%fused_computation.49 | convolution fusion | flops 2147483648 | bytes 8388608 | tf_op jit(solution)/shard_map/dot_general | solution.py:185
  258.5 10.0 %fusion.38 = bf16[512,2048]{1,0:T(8,128)(2,1)} fusion(bf16[1,1024,2048]{2,1,0:T(8,128)(2,1)} %param.35, f32[512,1024]{1,0:T(8,128)} %fusion.36, bf16[512,2048]{1,0:T(8,128)(2,1)S(1)} %bitcast.129, bf16[1,2048,1024]{2,1,0:T(8,128)(2,1)} %param.34), kind=kOutput, calls=%fused_computation.51 | convolution fusion | flops 4299161600 | bytes 14680064 | tf_op jit(solution)/shard_map/dot_general | solution.py:188
  268.5 4.6 %all-to-all-start.3 = ((bf16[32,16,2048]{2,1,0:T(8,128)(2,1)}), bf16[32,16,2048]{2,1,0:T(8,128)(2,1)S(1)}, u32[]{:S(2)}, u32[]{:S(2)}) async-start(bf16[32,16,2048]{2,1,0:T(8,128)(2,1)} %bitcast.127), calls=%async_computation.3 | async-start | bytes 4194304 | tf_op jit(solution)/shard_map/all_to_all | solution.py:189
  273.2 47.2 %all-to-all-done.3 = bf16[32,16,2048]{2,1,0:T(8,128)(2,1)S(1)} async-done(((bf16[32,16,2048]{2,1,0:T(8,128)(2,1)}), bf16[32,16,2048]{2,1,0:T(8,128)(2,1)S(1)}, u32[]{:S(2)}, u32[]{:S(2)}) %all-to-all-start.3) | async-done | bytes 2097184 | tf_op jit(solution)/shard_map/all_to_all | solution.py:189
  320.4 2.3 gather_fusion
  322.7 1.5 convert_element_type.66
  324.5 1.2 fusion.46
  (78 shorter events, 7.6 us)
Async XLA Ops:
  6.5 67.0 %all-gather.3.cloned.1.call-start = ((), (), s32[]{:S(2)}) async-start(), calls=%async_computation.4 | async-start | bytes 1114112 | tf_op jit(solution)/shard_map/all_gather | solution.py:136
  7.3 120.5 %all-gather.5.cloned.1.call-start = ((), (), s32[]{:S(2)}) async-start(), calls=%async_computation.5 | async-start | bytes 2228224 | tf_op jit(solution)/shard_map/all_gather | solution.py:137
  72.0 55.7 %copy-start.6 = (s32[256]{0:T(256)}, s32[256]{0:T(256)S(1)}, u32[]{:S(2)}) copy-start(s32[256]{0:T(256)S(1)} %fusion.58) | copy-start | bytes 3076
  130.5 5.0 %copy-start.3 = (f32[8,256]{1,0:T(8,128)S(1)}, f32[8,256]{1,0:T(8,128)}, u32[]{:S(2)}) copy-start(f32[8,256]{1,0:T(8,128)} %get-tuple-element.221) | copy-start | bytes 24580 | tf_op jit(solution)/shard_map/while/body/eval_jaxpr/cond
  141.6 5.6 %copy-start = (bf16[2,2048,256]{2,1,0:T(8,128)(2,1)S(1)}, bf16[2,2048,256]{2,1,0:T(8,128)(2,1)}, u32[]{:S(2)}) copy-start(bf16[2,2048,256]{2,1,0:T(8,128)(2,1)} %get-tuple-element.226) | copy-start | bytes 6291460 | tf_op jit(solution)/shard_map/while/body/eval_jaxpr/cond
  141.6 5.7 %copy-start.4 = (f32[4,256]{1,0:T(4,128)S(1)}, f32[4,256]{1,0:T(4,128)}, u32[]{:S(2)}) copy-start(f32[4,256]{1,0:T(4,128)} %get-tuple-element.228) | copy-start | bytes 12292 | tf_op jit(solution)/shard_map/while/body/eval_jaxpr/cond
  158.5 17.7 %copy-start.2 = (bf16[128,2048]{1,0:T(8,128)(2,1)S(1)}, bf16[128,2048]{1,0:T(8,128)(2,1)}, u32[]{:S(2)}) copy-start(bf16[128,2048]{1,0:T(8,128)(2,1)} %param.27) | copy-start | bytes 1572868
  158.5 17.7 %copy-start.8 = (f32[2048]{0:T(1024)S(1)}, f32[2048]{0:T(1024)}, u32[]{:S(2)}) copy-start(f32[2048]{0:T(1024)} %param.30) | copy-start | bytes 24580
  159.6 17.1 %copy-start.1 = (bf16[256,512]{1,0:T(8,128)(2,1)S(1)}, bf16[256,512]{1,0:T(8,128)(2,1)}, u32[]{:S(2)}) copy-start(bf16[256,512]{1,0:T(8,128)(2,1)} %fusion.53) | copy-start | bytes 786436
  159.6 17.1 %copy-start.9 = (f32[2048]{0:T(1024)S(1)}, f32[2048]{0:T(1024)}, u32[]{:S(2)}) copy-start(f32[2048]{0:T(1024)} %param.31) | copy-start | bytes 24580
  165.1 5.0 %all-to-all-start = ((bf16[2,128,512]{1,2,0:T(8,128)(2,1)}), bf16[2,128,512]{1,2,0:T(8,128)(2,1)S(1)}, u32[]{:S(2)}, u32[]{:S(2)}) async-start(bf16[2,128,512]{1,2,0:T(8,128)(2,1)} %copy.46), calls=%async_computation | async-start | bytes 524288 | tf_op jit(solution)/shard_map/all_to_all | solution.py:160
  173.0 81.9 %copy-start.11 = (bf16[1,2048,1024]{2,1,0:T(8,128)(2,1)S(1)}, bf16[1,2048,1024]{2,1,0:T(8,128)(2,1)}, u32[]{:S(2)}) copy-start(bf16[1,2048,1024]{2,1,0:T(8,128)(2,1)} %param.33) | copy-start | bytes 12582916
  258.5 14.6 %copy-start.5 = (s32[2,128]{1,0:T(2,128)S(1)}, s32[2,128]{1,0:T(2,128)}, u32[]{:S(2)}) copy-start(s32[2,128]{1,0:T(2,128)} %param.36) | copy-start | bytes 3076
  258.5 14.6 %copy-start.7 = (s32[256]{0:T(256)S(1)}, s32[256]{0:T(256)}, u32[]{:S(2)}) copy-start(s32[256]{0:T(256)} %copy-done.6) | copy-start | bytes 3076
  258.5 14.6 %copy-start.12 = (f32[128]{0:T(128)S(1)}, f32[128]{0:T(128)}, u32[]{:S(2)}) copy-start(f32[128]{0:T(128)} %param.37) | copy-start | bytes 1540
  268.5 51.8 %all-to-all-start.3 = ((bf16[32,16,2048]{2,1,0:T(8,128)(2,1)}), bf16[32,16,2048]{2,1,0:T(8,128)(2,1)S(1)}, u32[]{:S(2)}, u32[]{:S(2)}) async-start(bf16[32,16,2048]{2,1,0:T(8,128)(2,1)} %bitcast.127), calls=%async_computation.3 | async-start | bytes 4194304 | tf_op jit(solution)/shard_map/all_to_all | solution.py:189
  273.1 51.4 %copy-start.10 = (f32[2048]{0:T(1024)S(1)}, f32[2048]{0:T(1024)}, u32[]{:S(2)}) copy-start(f32[2048]{0:T(1024)} %param.32) | copy-start | bytes 24580
Sparse Core Ops, SparseCore 0:
  10.1 54.5 all-gather.2
  67.4 60.2 all-gather.4
where the time goes:
time: 336 us; the launch traced here: 333 us
  blocking collectives  141 us (42%)
  waiting for transfers between devices  102 us (30%)
  matrix products  36.9 us (11%)
  other arithmetic  18.1 us (5%)
  between operations  13.7 us (4%)
  local copies, waits for them, and re-layouts  8.6 us (3%)
  starting transfers between devices  8.4 us (2%)
    all_to_all x1, blocking collectives, on_device(): lax.all_to_all(outgoing, ('sp', 'tp'), split_axis=0, concat_axis=0, tiled...  77.4 us
    all_gather x1, waiting for transfers between devices, on_device(): lax.all_gather(kv_large, 'sp', axis=0, tiled=True)  52.7 us
    all_to_all x1, waiting for transfers between devices, on_device(): lax.all_to_all(expert_out.reshape(received.shape), ('sp', 'tp'), split_ax...  47.2 us
    all_gather x1, blocking collectives, on_device(): lax.all_gather(cum_small, 'sp', axis=1, tiled=True)  30.7 us
    all_gather x1, blocking collectives, on_device(): lax.all_gather(cum_large, 'sp', axis=1, tiled=True)  28 us
    dot_general x1, matrix products, on_device(): jnp.dot(hidden, w_down[0], preferred_element_type=jnp.float32)  9.98 us
    dot_general x2, matrix products, online_update(): jnp.einsum('hqk,kd->hqd', weights.astype(jnp.bfloat16), value_rows, prefe...  9.26 us
    reduce_sum x2, other arithmetic, online_update(): running_sum = running_sum * factor + jnp.sum(weights, axis=-1)  8.95 us
  transfers between devices with their start and end apart: 4, of which 3 were waited for; matrix products, arithmetic and copies ran while one was open for 3% of the time, Pallas kernels for 0%

commit v1 on v0

v1 whole, which is shorter than its diff:
```python
import functools
import math

import jax
import jax.numpy as jnp
from jax import lax
from jax.experimental import pallas as pl
from jax.experimental.pallas import tpu as pltpu
from jax.sharding import PartitionSpec as P

norm_eps = 1e-06
far_score = -1e30
log2e = math.log2(math.e)
MESH = pl.DeviceIdType.MESH


def rms_scale(values, gain_row):
    return (
        values * lax.rsqrt(jnp.mean(values * values, axis=-1, keepdims=True) + norm_eps) * gain_row
    )


def mesh_shape(mesh):
    coords = [tuple(device.coords) for device in mesh.devices.reshape(-1)]
    return tuple(1 + max(c[axis] for c in coords) - min(c[axis] for c in coords) for axis in (2, 1, 0))


def gather_kernel(dims, kv_ref, cum_ref, kv_all, cum_all, send_kv, send_cum, send_core, recv_kv, recv_cum, recv_core, own_sem):
    depth, rows_y, rows_x = dims
    plane = rows_y * rows_x
    me = lax.axis_index("sp")
    core = lax.axis_index("tp")
    mine_z = me // plane
    mine_y = me % plane // rows_x
    mine_x = me % rows_x
    half = kv_ref.shape[0] // 2
    barrier = pltpu.get_barrier_semaphore()
    peers = 0
    for step in range(1, depth):
        target = (mine_z + step) % depth * plane + me % plane
        pl.semaphore_signal(barrier, inc=1, device_id=(target, core), device_id_type=MESH)
        peers += 1
    for step in range(1, rows_y):
        target = mine_z * plane + (mine_y + step) % rows_y * rows_x + mine_x
        pl.semaphore_signal(barrier, inc=1, device_id=(target, core), device_id_type=MESH)
        peers += 1
    for step in range(1, rows_x):
        target = mine_z * plane + mine_y * rows_x + (mine_x + step) % rows_x
        pl.semaphore_signal(barrier, inc=1, device_id=(target, core), device_id_type=MESH)
        peers += 1
    pl.semaphore_signal(barrier, inc=1, device_id=(me, 1 - core), device_id_type=MESH)
    own_kv = pltpu.make_async_copy(kv_ref, kv_all.at[me], own_sem.at[0])
    own_cum = pltpu.make_async_copy(cum_ref, cum_all.at[me], own_sem.at[1])
    own_kv.start()
    own_cum.start()
    own_kv.wait()
    own_cum.wait()
    pl.semaphore_wait(barrier, peers + 1)

    def copies(shard, target, slot):
        part = kv_all.at[shard, pl.ds(core * half, half)]
        return (
            pltpu.make_async_remote_copy(
                src_ref=part, dst_ref=part, send_sem=send_kv.at[slot], recv_sem=recv_kv.at[shard],
                device_id=(target, core), device_id_type=MESH),
            pltpu.make_async_remote_copy(
                src_ref=cum_all.at[shard], dst_ref=cum_all.at[shard], send_sem=send_cum.at[slot],
                recv_sem=recv_cum.at[shard], device_id=(target, core), device_id_type=MESH),
        )

    def across(shard):
        part = kv_all.at[shard, pl.ds(core * half, half)]
        return pltpu.make_async_remote_copy(
            src_ref=part, dst_ref=part, send_sem=send_core.at[shard], recv_sem=recv_core.at[shard],
            device_id=(me, 1 - core), device_id_type=MESH)

    def arrived(shard):
        for copy in copies(shard, me, 0):
            copy.wait_recv()

    def other_half(shard):
        part = kv_all.at[shard, pl.ds((1 - core) * half, half)]
        return pltpu.make_async_remote_copy(
            src_ref=part, dst_ref=part, send_sem=send_core.at[shard], recv_sem=recv_core.at[shard],
            device_id=(me, 1 - core), device_id_type=MESH)

    def route(first_axis):
        size_a, size_b = (rows_y, rows_x) if first_axis == "y" else (rows_x, rows_y)
        here_a, here_b = (mine_y, mine_x) if first_axis == "y" else (mine_x, mine_y)

        def index(z, a, b):
            return z * plane + (a * rows_x + b if first_axis == "y" else b * rows_x + a)

        sends = []
        slot = 0
        for step in range(1, depth):
            sends.append((mine_z + step < depth, index(mine_z, here_a, here_b), index(mine_z + step, here_a, here_b), slot))
            slot += 1

        def start(items):
            for _, shard, target, number in items:
                for copy in copies(shard, target, number):
                    copy.start()

        for item in sends:
            pl.when(item[0])(functools.partial(start, [item]))
        for behind in range(depth):
            z = mine_z - behind
            items = []
            shard = index(z, here_a, here_b)
            for step in range(1, size_a):
                items.append((z >= 0, shard, index(mine_z, (here_a + step) % size_a, here_b), slot))
                slot += 1
            for step in range(1, size_b):
                items.append((z >= 0, shard, index(mine_z, here_a, (here_b + step) % size_b), slot))
                slot += 1
            sends += items

            def forward(items=items, shard=shard, behind=behind):
                if behind:
                    arrived(shard)
                start(items)
                if behind:
                    across(shard).start()

            pl.when(z >= 0)(forward)
        for behind in range(depth):
            z = mine_z - behind
            for step_a in range(1, size_a):
                shard = index(z, (here_a + size_a - step_a) % size_a, here_b)
                items = []
                for step in range(1, size_b):
                    items.append((z >= 0, shard, index(mine_z, here_a, (here_b + step) % size_b), slot))
                    slot += 1
                sends += items

                def relay(items=items, shard=shard):
                    arrived(shard)
                    start(items)
                    across(shard).start()

                pl.when(z >= 0)(relay)
        for behind in range(depth):
            z = mine_z - behind
            for step_b in range(1, size_b):
                for step_a in range(size_a):
                    shard = index(z, (here_a + size_a - step_a) % size_a, (here_b + size_b - step_b) % size_b)

                    def last(shard=shard):
                        arrived(shard)
                        across(shard).start()

                    pl.when(z >= 0)(last)
        for behind in range(depth):
            z = mine_z - behind

            def settle(z=z):
                for place in range(plane):

                    def finish_half(shard=z * plane + place):
                        other_half(shard).wait_recv()
                        across(shard).wait_send()

                    pl.when(z * plane + place != me)(finish_half)

            pl.when(z >= 0)(settle)
        for item in sends:

            def sent(item=item):
                for copy in copies(item[1], item[2], item[3]):
                    copy.wait_send()

            pl.when(item[0])(sent)

    pl.when(core == 0)(functools.partial(route, "y"))
    pl.when(core == 1)(functools.partial(route, "x"))


def gather_keys(dims, kv, cum):
    shards = lax.axis_size("sp")
    depth, rows_y, rows_x = dims
    slots = depth - 1 + depth * (rows_y + rows_x - 2) + depth * (rows_y - 1) * (rows_x - 1)
    dma = pltpu.SemaphoreType.DMA
    return pl.pallas_call(
        functools.partial(gather_kernel, dims),
        out_shape=(
            jax.ShapeDtypeStruct((shards,) + kv.shape, kv.dtype),
            jax.ShapeDtypeStruct((shards,) + cum.shape, cum.dtype),
        ),
        in_specs=[pl.BlockSpec(memory_space=pltpu.VMEM)] * 2,
        out_specs=(pl.BlockSpec(memory_space=pltpu.VMEM),) * 2,
        scratch_shapes=[
            dma((slots,)), dma((slots,)), dma((shards,)), dma((shards,)), dma((shards,)), dma((shards,)), dma((2,)),
        ],
        compiler_params=pltpu.CompilerParams(collective_id=0, has_side_effects=True),
        name="gather_keys",
    )(kv, cum)


def attend_kernel(head_shape, group, q_small, q_large, kv_all, cum_all, o_small, o_large, qs, ql, top, total, acc_s, acc_l):
    heads_small, heads_large, size_small, size_large = head_shape
    me = lax.axis_index("sp")
    tokens = q_small.shape[0]
    width = group * tokens
    for h in range(heads_small):
        qs[h] = q_small[:, h * size_small:(h + 1) * size_small]
    for h in range(heads_large):
        ql[h] = q_large[:, h * size_large:(h + 1) * size_large]
    top[...] = jnp.full_like(top, far_score)
    total[...] = jnp.zeros_like(total)
    acc_s[...] = jnp.zeros_like(acc_s)
    acc_l[...] = jnp.zeros_like(acc_l)

    def block(number, masked):
        first = number * group

        def run(heads, base, q_ref, acc_ref, column, size):
            scale = size ** (-0.5) * log2e

            def one(h, _):
                keys = kv_all[pl.ds(first, group), :, column:column + size].reshape(width, size)
                values = kv_all[pl.ds(first, group), :, column + size:column + 2 * size].reshape(width, size)
                gates = jnp.concatenate(
                    [cum_all[first + j, pl.ds(base + h, 1), :] for j in range(group)], axis=1
                ) * log2e
                scores = lax.dot_general(
                    q_ref[h], keys, (((1,), (1,)), ((), ())), preferred_element_type=jnp.float32
                ) * scale - gates
                if masked:
                    key_pos = lax.broadcasted_iota(jnp.int32, (tokens, width), 1) + first * tokens
                    query_pos = lax.broadcasted_iota(jnp.int32, (tokens, width), 0) + me * tokens
                    scores = jnp.where(key_pos <= query_pos, scores, far_score)
                before = top[base + h]
                newest = jnp.maximum(before, jnp.max(scores, axis=-1, keepdims=True))
                factor = jnp.exp2(before - newest)
                weights = jnp.exp2(scores - newest[:, :1])
                partial_sum = weights[:, :128]
                for j in range(1, width // 128):
                    partial_sum = partial_sum + weights[:, j * 128:(j + 1) * 128]
                top[base + h] = newest
                total[base + h] = total[base + h] * factor + partial_sum
                acc_ref[h] = acc_ref[h] * factor[:, :size] + jnp.dot(
                    weights.astype(jnp.bfloat16), values, preferred_element_type=jnp.float32
                )
                return 0

            lax.fori_loop(0, heads, one, 0)

        run(heads_small, 0, qs, acc_s, 0, size_small)
        run(heads_large, heads_small, ql, acc_l, 2 * size_small, size_large)

    last = me // group

    def whole(number, _):
        block(number, False)
        return 0

    lax.fori_loop(0, last, whole, 0)
    block(last, True)
    for h in range(heads_small):
        o_small[:, h * size_small:(h + 1) * size_small] = (
            acc_s[h] / jnp.sum(total[h], axis=-1, keepdims=True)
        ).astype(o_small.dtype)
    for h in range(heads_large):
        o_large[:, h * size_large:(h + 1) * size_large] = (
            acc_l[h] / jnp.sum(total[heads_small + h], axis=-1, keepdims=True)
        ).astype(o_large.dtype)


def attend(queries_small, queries_large, kv_all, cum_all, head_shape, group):
    heads_small, heads_large, size_small, size_large = head_shape
    tokens = queries_small.shape[0]
    heads = heads_small + heads_large
    return pl.pallas_call(
        functools.partial(attend_kernel, head_shape, group),
        out_shape=(
            jax.ShapeDtypeStruct(queries_small.shape, jnp.bfloat16),
            jax.ShapeDtypeStruct(queries_large.shape, jnp.bfloat16),
        ),
        in_specs=[pl.BlockSpec(memory_space=pltpu.VMEM)] * 4,
        out_specs=(pl.BlockSpec(memory_space=pltpu.VMEM),) * 2,
        scratch_shapes=[
            pltpu.VMEM((heads_small, tokens, size_small), jnp.bfloat16),
            pltpu.VMEM((heads_large, tokens, size_large), jnp.bfloat16),
            pltpu.VMEM((heads, tokens, 128), jnp.float32),
            pltpu.VMEM((heads, tokens, 128), jnp.float32),
            pltpu.VMEM((heads_small, tokens, size_small), jnp.float32),
            pltpu.VMEM((heads_large, tokens, size_large), jnp.float32),
        ],
        compiler_params=pltpu.CompilerParams(vmem_limit_bytes=56 * 1024 * 1024),
        name="attend",
    )(queries_small, queries_large, kv_all, cum_all)


def on_device(
    dims,
    queries_small,
    queries_large,
    kv_small,
    kv_large,
    cum_small,
    cum_large,
    residual,
    out_small,
    out_large,
    gain_mix,
    gain_route,
    gain_blend,
    w_gate,
    w_up,
    w_down,
    route,
    route_bias,
):
    tokens_here = queries_small.shape[0]
    heads_small = cum_small.shape[0]
    heads_large = cum_large.shape[0]
    size_small = kv_small.shape[1] // 2
    size_large = kv_large.shape[1] // 2
    kv_all, cum_all = gather_keys(
        dims,
        jnp.concatenate([kv_small, kv_large], axis=1),
        jnp.concatenate([cum_small, cum_large], axis=0),
    )
    group = math.gcd(dims[1] * dims[2], 4)
    attn_small, attn_large = attend(
        queries_small,
        queries_large,
        kv_all,
        cum_all,
        (heads_small, heads_large, size_small, size_large),
        group,
    )
    row_count = tokens_here // lax.axis_size("tp")
    whole_small, whole_large = (
        lax.all_to_all(attn_small, "tp", split_axis=0, concat_axis=1, tiled=True),
        lax.all_to_all(attn_large, "tp", split_axis=0, concat_axis=1, tiled=True),
    )
    mixer_out = jnp.dot(whole_small, out_small, preferred_element_type=jnp.float32) + jnp.dot(
        whole_large, out_large, preferred_element_type=jnp.float32
    )
    mixed = (residual.astype(jnp.float32) + rms_scale(mixer_out, gain_mix)).astype(jnp.bfloat16)
    routed = rms_scale(mixed.astype(jnp.float32), gain_route).astype(jnp.bfloat16)
    experts = lax.axis_size(("sp", "tp"))
    capacity = 4 * row_count // experts
    flat_ids = route.reshape(2 * row_count)
    marked = (flat_ids[:, None] == jnp.arange(experts, dtype=jnp.int32)[None, :]).astype(jnp.int32)
    ranked = jnp.sum((jnp.cumsum(marked, axis=0) - 1) * marked, axis=1)
    slot_ids = flat_ids * capacity + ranked
    dispatch_table = (
        slot_ids[:, None] == jnp.arange(experts * capacity, dtype=jnp.int32)[None, :]
    ).astype(jnp.bfloat16)
    dispatch_table = dispatch_table[:row_count] + dispatch_table[row_count:]
    outgoing = jnp.einsum(
        "rs,rd->sd", dispatch_table, routed, preferred_element_type=jnp.float32
    ).astype(jnp.bfloat16)
    outgoing = outgoing.reshape(experts, capacity, routed.shape[1])
    received = lax.all_to_all(outgoing, ("sp", "tp"), split_axis=0, concat_axis=0, tiled=True)
    row_total = received.shape[0] * received.shape[1]
    expert_rows = received.reshape(row_total, received.shape[2])
    gate_pre = jnp.dot(expert_rows, w_gate[0], preferred_element_type=jnp.float32)
    up_pre = jnp.dot(expert_rows, w_up[0], preferred_element_type=jnp.float32)
    hidden = (jax.nn.silu(gate_pre) * up_pre).astype(jnp.bfloat16)
    expert_out = jnp.dot(hidden, w_down[0], preferred_element_type=jnp.float32).astype(jnp.bfloat16)
    returned = lax.all_to_all(
        expert_out.reshape(received.shape), ("sp", "tp"), split_axis=0, concat_axis=0, tiled=True
    )
    picked = returned.reshape(experts * capacity, routed.shape[1])[slot_ids].astype(jnp.float32)
    blended = (
        jax.nn.sigmoid(route_bias)[:, None] * picked[:row_count]
        + jax.nn.sigmoid(-route_bias)[:, None] * picked[row_count:]
    )
    return (mixed.astype(jnp.float32) + rms_scale(blended, gain_blend)).astype(jnp.bfloat16)


def solution(mesh):
    in_specs = (
        P("sp", "tp"),
        P("sp", "tp"),
        P("sp", None),
        P("sp", None),
        P("tp", "sp"),
        P("tp", "sp"),
        P(("sp", "tp"), None),
        P(),
        P(),
        P(),
        P(),
        P(),
        P(("sp", "tp"), None, None),
        P(("sp", "tp"), None, None),
        P(("sp", "tp"), None, None),
        P(None, ("sp", "tp")),
        P(("sp", "tp")),
    )
    out_specs = P(("sp", "tp"), None)
    return jax.shard_map(
        functools.partial(on_device, mesh_shape(mesh)), mesh=mesh, in_specs=in_specs, out_specs=out_specs, check_vma=False
    )
```

time: 336 us -> 220 us (0.65)
  blocking collectives: 141 us -> 78.1 us
  waiting for transfers between devices: 102 us -> 47.2 us
  Pallas kernels: 0 us -> 45.7 us
  matrix products: 36.9 us -> 20.4 us
  between operations: 13.7 us -> 0.2 us
  other arithmetic: 18.1 us -> 7.16 us
    all_gather x2 -> x0, blocking collectives: 58.7 us -> none  [the longest x1 30.7 us: on_device(): lax.all_gather(cum_small, 'sp', axis=1, tiled=True)]
    all_gather x2 -> x0, waiting for transfers between devices: 52.7 us -> none  [the longest x1 52.7 us: on_device(): lax.all_gather(kv_large, 'sp', axis=0, tiled=True)]
    pallas_call x0 -> x2, Pallas kernels: none -> 45.7 us  [the longest x1 23.3 us: attend(): pl.pallas_call(functools.partial(attend_kernel, head_shape, group), out_s...]
    dot_general x4 -> x0, matrix products: 16.4 us -> none  [the longest x2 9.26 us: online_update(): jnp.einsum('hqk,kd->hqd', weights.astype(jnp.bfloat16), value_rows, prefe...]
    reduce_sum x2 -> x0, other arithmetic: 8.95 us -> none  [online_update(): running_sum = running_sum * factor + jnp.sum(weights, axis=-1)]
    all_to_all x1 -> x0, blocking collectives: 5.2 us -> none  [on_device(): lax.all_to_all(attn_large, 'tp', split_axis=0, concat_axis=1, tiled=True)]
    unnamed x24 -> x14, local copies, waits for them, and re-layouts: 3.87 us -> 0.28 us
    all_to_all x0 -> x1, starting transfers between devices: none -> 3.45 us  [on_device(): lax.all_to_all(attn_large, 'tp', split_axis=0, concat_axis=1, tiled=True)]
  transfers between devices with their start and end apart: 4 -> 3, of which waited for: 3 -> 1; matrix products, arithmetic and copies ran while one was open for 3% -> 2% of each run, Pallas kernels for 0% -> 0%
where the time goes in v1:
time: 220 us; the launch traced here: 217 us
  blocking collectives  78.1 us (35%)
  waiting for transfers between devices  47.2 us (21%)
  Pallas kernels  45.7 us (21%)
  matrix products  20.4 us (9%)
  starting transfers between devices  11.6 us (5%)
  other arithmetic  7.16 us (3%)
  local copies, waits for them, and re-layouts  6.38 us (3%)
    all_to_all x1, blocking collectives, on_device(): lax.all_to_all(outgoing, ('sp', 'tp'), split_axis=0, concat_axis=0, tiled...  78.1 us
    all_to_all x1, waiting for transfers between devices, on_device(): lax.all_to_all(expert_out.reshape(received.shape), ('sp', 'tp'), split_ax...  47.2 us
    pallas_call x1, Pallas kernels, attend(): pl.pallas_call(functools.partial(attend_kernel, head_shape, group), out_s...  23.3 us
    pallas_call x1, Pallas kernels, gather_keys(): pl.pallas_call(functools.partial(gather_kernel, dims), out_shape=(jax.Sha...  22.4 us
    dot_general x1, matrix products, on_device(): jnp.dot(hidden, w_down[0], preferred_element_type=jnp.float32)  9.89 us
    all_to_all x1, starting transfers between devices, on_device(): lax.all_to_all(expert_out.reshape(received.shape), ('sp', 'tp'), split_ax...  4.58 us
  transfers between devices with their start and end apart: 3, of which 1 were waited for; matrix products, arithmetic and copies ran while one was open for 2% of the time, Pallas kernels for 0%

profile of v1, /device:TPU:9, one launch (start us, length us, event | category | flops | bytes accessed | tf_op | source)
XLA Modules:
  0.0 216.8 jit_solution(5573848296702801059)
XLA Ops:
  0.0 1.6 pad_maximum_fusion.kv_ref
  1.6 1.3 pad_maximum_fusion.1.cum_ref
  2.9 22.4 %gather_keys.1 = (bf16[16,256,384]{2,1,0:T(8,128)(2,1)}, f32[16,12,256]{2,1,0:T(8,128)}) custom-call(bf16[256,384]{1,0:T(8,128)(2,1)} %pad_maximum_fusion.kv_ref, f32[12,256]{1,0:T(8,128)} %pad_maximum_fusion.1.cum_ref), custom_call_target="tpu_custom_call" | custom-call | tf_op jit(solution)/shard_map/gather_keys/pallas_call | solution.py:184
  25.4 23.3 %attend.1 = (bf16[256,512]{1,0:T(8,128)(2,1)}, bf16[256,512]{1,0:T(8,128)(2,1)}) custom-call(bf16[256,512]{1,0:T(8,128)(2,1)} %q_small.1, bf16[256,512]{1,0:T(8,128)(2,1)} %q_large.1, bf16[16,256,384]{2,1,0:T(8,128)(2,1)} %get-tuple-element.9.kv_all, f32[16,12,256]{2,1,0:T(8,128)} %get-tuple-element.10.cum_all), custom_call_target="tpu_custom_call" | custom-call | tf_op jit(solution)/shard_map/attend/pallas_call | solution.py:274
  48.6 1.8 copy.18
  50.4 3.6 %all-to-all-start = ((bf16[2,128,512]{1,2,0:T(8,128)(2,1)}), bf16[2,128,512]{1,2,0:T(8,128)(2,1)S(1)}, u32[]{:S(2)}, u32[]{:S(2)}) async-start(bf16[2,128,512]{1,2,0:T(8,128)(2,1)} %copy.18), calls=%async_computation | async-start | bytes 524288 | tf_op jit(solution)/shard_map/all_to_all | solution.py:336
  54.0 1.8 copy.19
  55.8 0.0 all-to-all-done
  55.8 3.5 %all-to-all-start.1 = ((bf16[2,128,512]{1,2,0:T(8,128)(2,1)}), bf16[2,128,512]{1,2,0:T(8,128)(2,1)S(1)}, u32[]{:S(2)}, u32[]{:S(2)}) async-start(bf16[2,128,512]{1,2,0:T(8,128)(2,1)} %copy.19), calls=%async_computation.1 | async-start | bytes 524288 | tf_op jit(solution)/shard_map/all_to_all | solution.py:337
  59.2 2.9 %fusion.27 = f32[128,2048]{1,0:T(8,128)S(1)} fusion(bf16[128,1024]{0,1:T(8,128)(2,1)S(1)} %bitcast.58, bf16[1024,2048]{1,0:T(8,128)(2,1)} %param.24), kind=kOutput, calls=%fused_computation.50 | convolution fusion | flops 536870912 | bytes 5505024 | tf_op jit(solution)/shard_map/dot_general | solution.py:339
  62.2 0.0 all-to-all-done.1
  62.2 0.0 copy-start
  62.2 0.0 copy-start.2
  62.2 3.1 %multiply_reduce_fusion.1 = (f32[128]{0:T(128)S(1)}, f32[128,2048]{1,0:T(8,128)S(1)}) fusion(f32[128,2048]{1,0:T(8,128)S(1)} %fusion.27, bf16[128,1024]{0,1:T(8,128)(2,1)S(1)} %bitcast.59, bf16[1024,2048]{1,0:T(8,128)(2,1)} %param.25), kind=kOutput, calls=%fused_computation.23 | convolution fusion | flops 537657216 | bytes 6554112 | tf_op jit(solution)/shard_map/dot_general | solution.py:339
  65.3 0.0 copy-start.3
  65.3 0.4 fusion.11
  65.7 0.2 copy-done.1
  66.0 0.6 reduce-window.6
  66.5 0.2 slice_reduce_fusion
  66.8 0.1 fusion.24
  66.9 0.1 fusion.21
  67.0 0.8 convolution_convert_fusion
  67.8 0.0 copy-start.5
  67.8 78.1 %all_to_all.48 = bf16[32,16,2048]{2,1,0:T(8,128)(2,1)S(1)} all-to-all(bf16[32,16,2048]{2,1,0:T(8,128)(2,1)S(1)} %bitcast.54), channel_id=1, replica_groups=mesh['sp'=16,'tp'=2] {'sp','tp'}, dimensions={0} | all-to-all | bytes 4194304 | tf_op jit(solution)/shard_map/all_to_all | solution.py:358
  146.0 3.7 %fusion.4 = f32[512,1024]{1,0:T(8,128)} fusion(bf16[512,2048]{1,0:T(8,128)(2,1)S(1)} %bitcast.56, bf16[1,2048,1024]{2,1,0:T(8,128)(2,1)S(1)} %copy-done.5), kind=kOutput, calls=%fused_computation.5 | convolution fusion | flops 2147483648 | bytes 8388608 | tf_op jit(solution)/shard_map/dot_general | solution.py:361
  149.7 9.9 %fusion.6 = bf16[512,2048]{1,0:T(8,128)(2,1)} fusion(bf16[1,1024,2048]{2,1,0:T(8,128)(2,1)} %param.31, f32[512,1024]{1,0:T(8,128)} %fusion.4, bf16[512,2048]{1,0:T(8,128)(2,1)S(1)} %bitcast.57, bf16[1,2048,1024]{2,1,0:T(8,128)(2,1)} %param.30), kind=kOutput, calls=%fused_computation.7 | convolution fusion | flops 4299161600 | bytes 14680064 | tf_op jit(solution)/shard_map/dot_general | solution.py:364
  159.6 4.6 %all-to-all-start.3 = ((bf16[32,16,2048]{2,1,0:T(8,128)(2,1)}), bf16[32,16,2048]{2,1,0:T(8,128)(2,1)S(1)}, u32[]{:S(2)}, u32[]{:S(2)}) async-start(bf16[32,16,2048]{2,1,0:T(8,128)(2,1)} %bitcast.55), calls=%async_computation.3 | async-start | bytes 4194304 | tf_op jit(solution)/shard_map/all_to_all | solution.py:365
  164.2 47.2 %all-to-all-done.3 = bf16[32,16,2048]{2,1,0:T(8,128)(2,1)S(1)} async-done(((bf16[32,16,2048]{2,1,0:T(8,128)(2,1)}), bf16[32,16,2048]{2,1,0:T(8,128)(2,1)S(1)}, u32[]{:S(2)}, u32[]{:S(2)}) %all-to-all-start.3) | async-done | bytes 2097184 | tf_op jit(solution)/shard_map/all_to_all | solution.py:365
  211.4 2.3 %gather_fusion = bf16[256,2048]{1,0:T(8,128)(2,1)} fusion(bf16[512,2048]{1,0:T(8,128)(2,1)S(1)} %bitcast.53, s32[1024]{0:T(1024)S(1)} %pad_clamp_fusion), kind=kCustom, calls=%fused_computation | custom fusion | bytes 2098176 | tf_op jit(solution)/shard_map/gather | solution.py:368
  213.8 1.5 convert_element_type.45
  215.2 0.3 multiply_reduce_fusion
  215.6 1.2 fusion.14
  (20 shorter events, 0.1 us)
Async XLA Ops:
  50.4 5.4 %all-to-all-start = ((bf16[2,128,512]{1,2,0:T(8,128)(2,1)}), bf16[2,128,512]{1,2,0:T(8,128)(2,1)S(1)}, u32[]{:S(2)}, u32[]{:S(2)}) async-start(bf16[2,128,512]{1,2,0:T(8,128)(2,1)} %copy.18), calls=%async_computation | async-start | bytes 524288 | tf_op jit(solution)/shard_map/all_to_all | solution.py:336
  55.8 6.4 %all-to-all-start.1 = ((bf16[2,128,512]{1,2,0:T(8,128)(2,1)}), bf16[2,128,512]{1,2,0:T(8,128)(2,1)S(1)}, u32[]{:S(2)}, u32[]{:S(2)}) async-start(bf16[2,128,512]{1,2,0:T(8,128)(2,1)} %copy.19), calls=%async_computation.1 | async-start | bytes 524288 | tf_op jit(solution)/shard_map/all_to_all | solution.py:337
  62.2 3.1 %copy-start = (bf16[128,2048]{1,0:T(8,128)(2,1)S(1)}, bf16[128,2048]{1,0:T(8,128)(2,1)}, u32[]{:S(2)}) copy-start(bf16[128,2048]{1,0:T(8,128)(2,1)} %param.23) | copy-start | bytes 1572868
  62.2 3.1 %copy-start.2 = (f32[2048]{0:T(1024)S(1)}, f32[2048]{0:T(1024)}, u32[]{:S(2)}) copy-start(f32[2048]{0:T(1024)} %param.26) | copy-start | bytes 24580
  65.3 0.7 copy-start.1
  65.3 1.7 copy-start.3
  67.8 78.1 %copy-start.5 = (bf16[1,2048,1024]{2,1,0:T(8,128)(2,1)S(1)}, bf16[1,2048,1024]{2,1,0:T(8,128)(2,1)}, u32[]{:S(2)}) copy-start(bf16[1,2048,1024]{2,1,0:T(8,128)(2,1)} %param.29) | copy-start | bytes 12582916
  159.6 4.6 %copy-start.6 = (f32[128]{0:T(128)S(1)}, f32[128]{0:T(128)}, u32[]{:S(2)}) copy-start(f32[128]{0:T(128)} %param.33) | copy-start | bytes 1540
  159.6 51.8 %all-to-all-start.3 = ((bf16[32,16,2048]{2,1,0:T(8,128)(2,1)}), bf16[32,16,2048]{2,1,0:T(8,128)(2,1)S(1)}, u32[]{:S(2)}, u32[]{:S(2)}) async-start(bf16[32,16,2048]{2,1,0:T(8,128)(2,1)} %bitcast.55), calls=%async_computation.3 | async-start | bytes 4194304 | tf_op jit(solution)/shard_map/all_to_all | solution.py:365
  213.8 1.8 copy-start.4

commit v2 on v1

--- a/solution.py
+++ b/solution.py
@@ -292,6 +292,247 @@
     )(queries_small, queries_large, kv_all, cum_all)
 
 
+def greet(depth, plane, cores, me, core):
+    barrier = pltpu.get_barrier_semaphore()
+    lanes = plane * cores
+    here = me % plane * cores + core
+    for step in range(1, depth):
+        target = (me // plane + step) % depth * plane + me % plane
+        pl.semaphore_signal(barrier, inc=1, device_id=(target, core), device_id_type=MESH)
+    for step in range(1, lanes):
+        other = (here + step) % lanes
+        target = me // plane * plane + other // cores
+        pl.semaphore_signal(barrier, inc=1, device_id=(target, other % cores), device_id_type=MESH)
+    pl.semaphore_wait(barrier, depth - 1 + lanes - 1)
+
+
+def distances(depth):
+    found = [0]
+    for step in range(1, depth):
+        found += [step, -step]
+    return found
+
+
+def dispatch_kernel(depth, cores, rows_ref, meta_ref, received, metas, in_rows, stage, send_rows, send_meta, recv_rows, recv_meta, send_block, recv_block, own_sem):
+    me = lax.axis_index("sp")
+    core = lax.axis_index("tp")
+    _, lanes, capacity, columns = stage.shape
+    plane = lanes // cores
+    slots = rows_ref.shape[1]
+    mine = me // plane
+    here = me % plane * cores + core
+    own_rows = pltpu.make_async_copy(rows_ref.at[mine], in_rows.at[mine], own_sem.at[0, 0])
+    own_meta = pltpu.make_async_copy(meta_ref.at[mine], metas.at[mine], own_sem.at[0, 1])
+    own_rows.start()
+    own_meta.start()
+    greet(depth, plane, cores, me, core)
+
+    def along(other):
+        target = (other * plane + me % plane, core)
+        return (
+            pltpu.make_async_remote_copy(
+                src_ref=rows_ref.at[other], dst_ref=in_rows.at[mine], send_sem=send_rows.at[other],
+                recv_sem=recv_rows.at[mine], device_id=target, device_id_type=MESH),
+            pltpu.make_async_remote_copy(
+                src_ref=meta_ref.at[other], dst_ref=metas.at[mine], send_sem=send_meta.at[other],
+                recv_sem=recv_meta.at[mine], device_id=target, device_id_type=MESH),
+        )
+
+    def incoming(other):
+        target = (other * plane + me % plane, core)
+        return (
+            pltpu.make_async_remote_copy(
+                src_ref=rows_ref.at[other], dst_ref=in_rows.at[other], send_sem=send_rows.at[other],
+                recv_sem=recv_rows.at[other], device_id=target, device_id_type=MESH),
+            pltpu.make_async_remote_copy(
+                src_ref=meta_ref.at[other], dst_ref=metas.at[other], send_sem=send_meta.at[other],
+                recv_sem=recv_meta.at[other], device_id=target, device_id_type=MESH),
+        )
+
+    def block(source, other, slot_of):
+        return pltpu.make_async_remote_copy(
+            src_ref=stage.at[source, other], dst_ref=received.at[source * lanes + slot_of],
+            send_sem=send_block.at[source, other], recv_sem=recv_block.at[source, slot_of],
+            device_id=(mine * plane + other // cores, other % cores), device_id_type=MESH)
+
+    def keep(source):
+        return pltpu.make_async_copy(
+            stage.at[source, here], received.at[source * lanes + here], own_sem.at[1, source])
+
+    steps = distances(depth)
+    for step in steps[1:]:
+        other = mine + step
+
+        def launch(other=other):
+            for copy in along(other):
+                copy.start()
+
+        pl.when((other >= 0) & (other < depth))(launch)
+    own_rows.wait()
+    own_meta.wait()
+    for step in steps:
+        other = mine + step
+
+        def expand(other=other, step=step):
+            if step:
+                for copy in incoming(other):
+                    copy.wait_recv()
+            wanted = lax.broadcasted_iota(jnp.int32, (lanes * capacity, slots), 0).astype(jnp.float32) + 1.0
+            first = metas[other, 0:1, :slots]
+            second = metas[other, 1:2, :slots]
+            table = jnp.where((wanted == first) | (wanted == second), 1.0, 0.0).astype(jnp.bfloat16)
+            spread = jnp.dot(table, in_rows[other], preferred_element_type=jnp.float32)
+            for lane in range(lanes):
+                stage[other, lane] = spread[lane * capacity:(lane + 1) * capacity].astype(jnp.bfloat16)
+            for move in range(1, lanes):
+                block(other, (here + move) % lanes, here).start()
+            keep(other).start()
+
+        pl.when((other >= 0) & (other < depth))(expand)
+    for source in range(depth):
+        keep(source).wait()
+        for move in range(1, lanes):
+            block(source, (here + move) % lanes, (here + move) % lanes).wait_recv()
+            block(source, (here + move) % lanes, here).wait_send()
+    for step in steps[1:]:
+        other = mine + step
+
+        def sent(other=other):
+            for copy in along(other):
+                copy.wait_send()
+
+        pl.when((other >= 0) & (other < depth))(sent)
+
+
+def dispatch(rows, meta, lanes, cores, capacity):
+    depth, slots, columns = rows.shape
+    dma = pltpu.SemaphoreType.DMA
+    vmem = pl.BlockSpec(memory_space=pltpu.VMEM)
+    return pl.pallas_call(
+        functools.partial(dispatch_kernel, depth, cores),
+        out_shape=(
+            jax.ShapeDtypeStruct((depth * lanes, capacity, columns), rows.dtype),
+            jax.ShapeDtypeStruct(meta.shape, meta.dtype),
+        ),
+        in_specs=[vmem] * 2,
+        out_specs=(vmem,) * 2,
+        scratch_shapes=[
+            pltpu.VMEM(rows.shape, rows.dtype),
+            pltpu.VMEM((depth, lanes, capacity, columns), rows.dtype),
+            dma((depth,)), dma((depth,)), dma((depth,)), dma((depth,)),
+            dma((depth, lanes)), dma((depth, lanes)), dma((2, max(depth, 2))),
+        ],
+        compiler_params=pltpu.CompilerParams(
+            collective_id=1, has_side_effects=True, vmem_limit_bytes=48 * 1024 * 1024),
+        name="dispatch_rows",
+    )(rows, meta)
+
+
+def return_kernel(depth, cores, outs, metas, final, back, stage, send_block, recv_block, send_rows, recv_rows, own_sem):
+    me = lax.axis_index("sp")
+    core = lax.axis_index("tp")
+    _, lanes, capacity, columns = back.shape
+    plane = lanes // cores
+    slots = final.shape[1]
+    mine = me // plane
+    here = me % plane * cores + core
+    greet(depth, plane, cores, me, core)
+
+    def block(source, other, slot_of):
+        return pltpu.make_async_remote_copy(
+            src_ref=outs.at[source * lanes + other], dst_ref=back.at[source, slot_of],
+            send_sem=send_block.at[source, other], recv_sem=recv_block.at[source, slot_of],
+            device_id=(mine * plane + other // cores, other % cores), device_id_type=MESH)
+
+    def keep(source):
+        return pltpu.make_async_copy(
+            outs.at[source * lanes + here], back.at[source, here], own_sem.at[source])
+
+    def along(other, slot_of):
+        return pltpu.make_async_remote_copy(
+            src_ref=stage.at[other], dst_ref=final.at[slot_of], send_sem=send_rows.at[other],
+            recv_sem=recv_rows.at[slot_of], device_id=(other * plane + me % plane, core), device_id_type=MESH)
+
+    steps = distances(depth)[::-1]
+    for step in steps:
+        other = mine + step
+
+        def launch(other=other):
+            for move in range(1, lanes):
+                block(other, (here + move) % lanes, here).start()
+            keep(other).start()
+
+        pl.when((other >= 0) & (other < depth))(launch)
+    for step in steps:
+        other = mine + step
+
+        def combine(other=other, step=step):
+            keep(other).wait()
+            for move in range(1, lanes):
+                block(other, (here + move) % lanes, (here + move) % lanes).wait_recv()
+            count = lanes * capacity
+            width = metas.shape[2]
+            wanted = lax.broadcasted_iota(jnp.int32, (count, width), 0).astype(jnp.float32) + 1.0
+            weights = jnp.where(wanted == metas[other, 0:1, :], metas[other, 2:3, :], 0.0)
+            weights = weights + jnp.where(wanted == metas[other, 1:2, :], metas[other, 3:4, :], 0.0)
+            weights = weights.T[:slots]
+            high = weights.astype(jnp.bfloat16)
+            low = (weights - high.astype(jnp.float32)).astype(jnp.bfloat16)
+            if capacity % 16:
+                picked = jnp.concatenate(
+                    [back[other, lane].astype(jnp.float32) for lane in range(lanes)], axis=0
+                ).astype(jnp.bfloat16)
+            else:
+                picked = back[other].reshape(count, columns)
+            mixed = jnp.dot(high, picked, preferred_element_type=jnp.float32) + jnp.dot(
+                low, picked, preferred_element_type=jnp.float32)
+            if step:
+                stage[other] = mixed.astype(stage.dtype)
+                along(other, mine).start()
+            else:
+                final[other] = mixed.astype(final.dtype)
+
+        pl.when((other >= 0) & (other < depth))(combine)
+    for step in steps:
+        other = mine + step
+
+        def settle(other=other, step=step):
+            for move in range(1, lanes):
+                block(other, (here + move) % lanes, here).wait_send()
+            if step:
+                along(other, other).wait_recv()
+                along(other, mine).wait_send()
+
+        pl.when((other >= 0) & (other < depth))(settle)
+
+
+def give_back(outs, metas, lanes, cores, slots):
+    depth = metas.shape[0]
+    _, capacity, columns = outs.shape
+    dma = pltpu.SemaphoreType.DMA
+    vmem = pl.BlockSpec(memory_space=pltpu.VMEM)
+    return pl.pallas_call(
+        functools.partial(return_kernel, depth, cores),
+        out_shape=jax.ShapeDtypeStruct((depth, slots, columns), outs.dtype),
+        in_specs=[vmem] * 2,
+        out_specs=vmem,
+        scratch_shapes=[
+            pltpu.VMEM((depth, lanes, capacity, columns), outs.dtype),
+            pltpu.VMEM((depth, slots, columns), outs.dtype),
+            dma((depth, lanes)), dma((depth, lanes)), dma((depth,)), dma((depth,)), dma((depth,)),
+        ],
+        compiler_params=pltpu.CompilerParams(
+            collective_id=2, has_side_effects=True, vmem_limit_bytes=48 * 1024 * 1024),
+        name="return_rows",
+    )(outs, metas)
+
+
+def earlier_same(ids):
+    order = jnp.arange(ids.shape[0], dtype=jnp.int32)
+    same = (ids[:, None] == ids[None, :]) & (order[None, :] < order[:, None])
+    return jnp.sum(same.astype(jnp.int32), axis=1)
+
+
 def on_device(
     dims,
     queries_small,
@@ -342,33 +583,40 @@
     mixed = (residual.astype(jnp.float32) + rms_scale(mixer_out, gain_mix)).astype(jnp.bfloat16)
     routed = rms_scale(mixed.astype(jnp.float32), gain_route).astype(jnp.bfloat16)
     experts = lax.axis_size(("sp", "tp"))
+    cores = lax.axis_size("tp")
+    depth = dims[0]
+    lanes = experts // depth
     capacity = 4 * row_count // experts
+    slots = capacity * lanes // 2
+    group_ids = route[0] // lanes
+    row_slots = group_ids * slots + earlier_same(group_ids)
+    row_table = row_slots[None, :] == jnp.arange(depth * slots, dtype=jnp.int32)[:, None]
     flat_ids = route.reshape(2 * row_count)
-    marked = (flat_ids[:, None] == jnp.arange(experts, dtype=jnp.int32)[None, :]).astype(jnp.int32)
-    ranked = jnp.sum((jnp.cumsum(marked, axis=0) - 1) * marked, axis=1)
-    slot_ids = flat_ids * capacity + ranked
-    dispatch_table = (
-        slot_ids[:, None] == jnp.arange(experts * capacity, dtype=jnp.int32)[None, :]
+    places = (flat_ids % lanes * capacity + earlier_same(flat_ids) + 1).astype(jnp.float32)
+    facts = jnp.stack(
+        [places[:row_count], places[row_count:], jax.nn.sigmoid(route_bias), jax.nn.sigmoid(-route_bias)]
+    )
+    meta = jnp.sum(jnp.where(row_table[None], facts[:, None, :], 0.0), axis=2)
+    meta = meta.reshape(4, depth, slots).transpose(1, 0, 2)
+    meta = jnp.pad(meta, ((0, 0), (0, 4), (0, -slots % 128)))
+    outgoing = jnp.dot(
+        row_table.astype(jnp.bfloat16), routed, preferred_element_type=jnp.float32
     ).astype(jnp.bfloat16)
-    dispatch_table = dispatch_table[:row_count] + dispatch_table[row_count:]
-    outgoing = jnp.einsum(
-        "rs,rd->sd", dispatch_table, routed, preferred_element_type=jnp.float32
-    ).astype(jnp.bfloat16)
-    outgoing = outgoing.reshape(experts, capacity, routed.shape[1])
-    received = lax.all_to_all(outgoing, ("sp", "tp"), split_axis=0, concat_axis=0, tiled=True)
+    received, metas = dispatch(
+        outgoing.reshape(depth, slots, routed.shape[1]), meta, lanes, cores, capacity
+    )
     row_total = received.shape[0] * received.shape[1]
     expert_rows = received.reshape(row_total, received.shape[2])
     gate_pre = jnp.dot(expert_rows, w_gate[0], preferred_element_type=jnp.float32)
     up_pre = jnp.dot(expert_rows, w_up[0], preferred_element_type=jnp.float32)
     hidden = (jax.nn.silu(gate_pre) * up_pre).astype(jnp.bfloat16)
     expert_out = jnp.dot(hidden, w_down[0], preferred_element_type=jnp.float32).astype(jnp.bfloat16)
-    returned = lax.all_to_all(
-        expert_out.reshape(received.shape), ("sp", "tp"), split_axis=0, concat_axis=0, tiled=True
-    )
-    picked = returned.reshape(experts * capacity, routed.shape[1])[slot_ids].astype(jnp.float32)
-    blended = (
-        jax.nn.sigmoid(route_bias)[:, None] * picked[:row_count]
-        + jax.nn.sigmoid(-route_bias)[:, None] * picked[row_count:]
+    returned = give_back(expert_out.reshape(received.shape), metas, lanes, cores, slots)
+    blended = lax.dot_general(
+        row_table.astype(jnp.bfloat16),
+        returned.reshape(depth * slots, routed.shape[1]),
+        (((0,), (0,)), ((), ())),
+        preferred_element_type=jnp.float32,
     )
     return (mixed.astype(jnp.float32) + rms_scale(blended, gain_blend)).astype(jnp.bfloat16)
 

time: 220 us -> 184 us (0.84); the launches traced: 217 us -> 184 us
  Pallas kernels: 45.7 us -> 147 us
  blocking collectives: 78.1 us -> 0 us
  waiting for transfers between devices: 47.2 us -> 0.01 us
  starting transfers between devices: 11.6 us -> 7.05 us
    pallas_call x0 -> x2, Pallas kernels: none -> 101 us  [the longest x1 55 us: dispatch(): pl.pallas_call(functools.partial(dispatch_kernel, depth, cores), out_shap...]
    all_to_all x1 -> x0, blocking collectives: 78.1 us -> none  [on_device(): lax.all_to_all(outgoing, ('sp', 'tp'), split_axis=0, concat_axis=0, tiled...]
    all_to_all x1 -> x0, waiting for transfers between devices: 47.2 us -> none  [on_device(): lax.all_to_all(expert_out.reshape(received.shape), ('sp', 'tp'), split_ax...]
    all_to_all x1 -> x0, starting transfers between devices: 4.58 us -> none  [on_device(): lax.all_to_all(expert_out.reshape(received.shape), ('sp', 'tp'), split_ax...]
    gather x1 -> x0, local copies, waits for them, and re-layouts: 2.35 us -> none  [on_device(): returned.reshape(experts * capacity, routed.shape[1])[slot_ids]]
  transfers between devices with their start and end apart: 3 -> 2, of which waited for: 1 -> 0; matrix products, arithmetic and copies ran while one was open for 2% -> 3% of each run, Pallas kernels for 0% -> 0%
where the time goes in v2:
time: 184 us
  Pallas kernels  147 us (80%)
  matrix products  19.9 us (11%)
  starting transfers between devices  7.05 us (4%)
  other arithmetic  5.04 us (3%)
  local copies, waits for them, and re-layouts  5 us (3%)
    pallas_call x1, Pallas kernels, dispatch(): pl.pallas_call(functools.partial(dispatch_kernel, depth, cores), out_shap...  55 us
    pallas_call x1, Pallas kernels, give_back(): pl.pallas_call(functools.partial(return_kernel, depth, cores), out_shape=...  46.1 us
    pallas_call x1, Pallas kernels, attend(): pl.pallas_call(functools.partial(attend_kernel, head_shape, group), out_s...  23.2 us
    pallas_call x1, Pallas kernels, gather_keys(): pl.pallas_call(functools.partial(gather_kernel, dims), out_shape=(jax.Sha...  22.4 us
    dot_general x1, matrix products, on_device(): jnp.dot(hidden, w_down[0], preferred_element_type=jnp.float32)  9.23 us
    dot_general x1, matrix products, on_device(): jnp.dot(expert_rows, w_gate[0], preferred_element_type=jnp.float32)  3.69 us
  transfers between devices with their start and end apart: 2, of which 0 were waited for; matrix products, arithmetic and copies ran while one was open for 3% of the time, Pallas kernels for 0%

profile of v2, /device:TPU:9, one launch (start us, length us, event | category | flops | bytes accessed | tf_op | source)
XLA Modules:
  0.0 183.9 jit_solution(9319980739967119718)
XLA Ops:
  0.0 1.3 pad_maximum_fusion.1.cum_ref
  1.3 1.6 pad_maximum_fusion.kv_ref
  3.0 22.4 %gather_keys.1 = (bf16[16,256,384]{2,1,0:T(8,128)(2,1)}, f32[16,12,256]{2,1,0:T(8,128)}) custom-call(bf16[256,384]{1,0:T(8,128)(2,1)} %pad_maximum_fusion.kv_ref, f32[12,256]{1,0:T(8,128)} %pad_maximum_fusion.1.cum_ref), custom_call_target="tpu_custom_call" | custom-call | tf_op jit(solution)/shard_map/gather_keys/pallas_call | solution.py:184
  25.4 23.2 %attend.1 = (bf16[256,512]{1,0:T(8,128)(2,1)}, bf16[256,512]{1,0:T(8,128)(2,1)}) custom-call(bf16[256,512]{1,0:T(8,128)(2,1)} %q_small.1, bf16[256,512]{1,0:T(8,128)(2,1)} %q_large.1, bf16[16,256,384]{2,1,0:T(8,128)(2,1)} %get-tuple-element.11.kv_all, f32[16,12,256]{2,1,0:T(8,128)} %get-tuple-element.12.cum_all), custom_call_target="tpu_custom_call" | custom-call | tf_op jit(solution)/shard_map/attend/pallas_call | solution.py:274
  48.7 1.8 copy.21
  50.4 3.6 %all-to-all-start = ((bf16[2,128,512]{1,2,0:T(8,128)(2,1)}), bf16[2,128,512]{1,2,0:T(8,128)(2,1)S(1)}, u32[]{:S(2)}, u32[]{:S(2)}) async-start(bf16[2,128,512]{1,2,0:T(8,128)(2,1)} %copy.21), calls=%async_computation | async-start | bytes 524288 | tf_op jit(solution)/shard_map/all_to_all | solution.py:577
  54.0 0.0 copy-done.2
  54.0 0.2 convert_reduce_fusion.1
  54.2 0.2 convert_reduce_fusion
  54.5 0.2 select_reduce_fusion
  54.7 0.1 reshape.107
  54.8 1.8 copy.22
  56.6 0.0 all-to-all-done
  56.6 3.5 %all-to-all-start.1 = ((bf16[2,128,512]{1,2,0:T(8,128)(2,1)}), bf16[2,128,512]{1,2,0:T(8,128)(2,1)S(1)}, u32[]{:S(2)}, u32[]{:S(2)}) async-start(bf16[2,128,512]{1,2,0:T(8,128)(2,1)} %copy.22), calls=%async_computation.1 | async-start | bytes 524288 | tf_op jit(solution)/shard_map/all_to_all | solution.py:578
  60.1 2.9 %fusion.30 = f32[128,2048]{1,0:T(8,128)S(1)} fusion(bf16[128,1024]{0,1:T(8,128)(2,1)S(1)} %bitcast.68, bf16[1024,2048]{1,0:T(8,128)(2,1)} %param.24), kind=kOutput, calls=%fused_computation.63 | convolution fusion | flops 536870912 | bytes 5505024 | tf_op jit(solution)/shard_map/dot_general | solution.py:580
  63.0 0.0 all-to-all-done.1
  63.0 0.0 copy-start.1
  63.0 0.0 copy-start.3
  63.1 0.0 copy-start.4
  63.1 3.1 %multiply_reduce_fusion.1 = (f32[128]{0:T(128)S(1)}, f32[128,2048]{1,0:T(8,128)S(1)}) fusion(f32[128,2048]{1,0:T(8,128)S(1)} %fusion.30, bf16[128,1024]{0,1:T(8,128)(2,1)S(1)} %bitcast.69, bf16[1024,2048]{1,0:T(8,128)(2,1)} %param.25), kind=kOutput, calls=%fused_computation.19 | convolution fusion | flops 537657216 | bytes 6554112 | tf_op jit(solution)/shard_map/dot_general | solution.py:580
  66.1 0.0 copy-start.7
  66.2 0.4 fusion.11
  66.6 0.5 convolution_convert_fusion
  67.1 55.0 %dispatch_rows.1 = (bf16[32,16,2048]{2,1,0:T(8,128)(2,1)S(1)}, f32[4,8,128]{2,1,0:T(8,128)S(1)}) custom-call(bf16[4,64,2048]{2,1,0:T(8,128)(2,1)S(1)} %bitcast.64, f32[4,8,128]{2,1,0:T(8,128)S(1)} %pad.4.meta_ref), custom_call_target="tpu_custom_call" | custom-call | tf_op jit(solution)/shard_map/dispatch_rows/pallas_call | solution.py:411
  122.1 0.0 copy-start
  122.1 1.3 copy-done
  123.4 3.7 %fusion.4 = f32[512,1024]{1,0:T(8,128)} fusion(bf16[512,2048]{1,0:T(8,128)(2,1)S(1)} %bitcast.66, bf16[1,2048,1024]{2,1,0:T(8,128)(2,1)S(1)} %copy-done.7), kind=kOutput, calls=%fused_computation.4 | convolution fusion | flops 2147483648 | bytes 8388608 | tf_op jit(solution)/shard_map/dot_general | solution.py:610
  127.1 9.2 %fusion.6 = bf16[512,2048]{1,0:T(8,128)(2,1)S(1)} fusion(bf16[1,1024,2048]{2,1,0:T(8,128)(2,1)} %param.31, f32[512,1024]{1,0:T(8,128)} %fusion.4, bf16[512,2048]{1,0:T(8,128)(2,1)} %bitcast.67, bf16[1,2048,1024]{2,1,0:T(8,128)(2,1)} %param.30), kind=kOutput, calls=%fused_computation.6 | convolution fusion | flops 4299161600 | bytes 14680064 | tf_op jit(solution)/shard_map/dot_general | solution.py:613
  136.3 0.0 copy-start.5
  136.3 46.1 %return_rows.1 = bf16[4,64,2048]{2,1,0:T(8,128)(2,1)S(1)} custom-call(bf16[32,16,2048]{2,1,0:T(8,128)(2,1)S(1)} %bitcast.65, f32[4,8,128]{2,1,0:T(8,128)S(1)} %get-tuple-element.16.metas), custom_call_target="tpu_custom_call" | custom-call | tf_op jit(solution)/shard_map/return_rows/pallas_call | solution.py:514
  182.4 0.4 multiply_reduce_fusion
  182.9 1.0 fusion.14
  (20 shorter events, 0.1 us)
Async XLA Ops:
  0.0 54.0 %copy-start.2 = (s32[2,128]{1,0:T(2,128)S(1)}, s32[2,128]{1,0:T(2,128)}, u32[]{:S(2)}) copy-start(s32[2,128]{1,0:T(2,128)} %param.32) | copy-start | bytes 3076
  0.0 54.5 %copy-start.6 = (f32[128]{0:T(128)S(1)}, f32[128]{0:T(128)}, u32[]{:S(2)}) copy-start(f32[128]{0:T(128)} %param.33) | copy-start | bytes 1540
  50.4 6.2 %all-to-all-start = ((bf16[2,128,512]{1,2,0:T(8,128)(2,1)}), bf16[2,128,512]{1,2,0:T(8,128)(2,1)S(1)}, u32[]{:S(2)}, u32[]{:S(2)}) async-start(bf16[2,128,512]{1,2,0:T(8,128)(2,1)} %copy.21), calls=%async_computation | async-start | bytes 524288 | tf_op jit(solution)/shard_map/all_to_all | solution.py:577
  56.6 6.4 %all-to-all-start.1 = ((bf16[2,128,512]{1,2,0:T(8,128)(2,1)}), bf16[2,128,512]{1,2,0:T(8,128)(2,1)S(1)}, u32[]{:S(2)}, u32[]{:S(2)}) async-start(bf16[2,128,512]{1,2,0:T(8,128)(2,1)} %copy.22), calls=%async_computation.1 | async-start | bytes 524288 | tf_op jit(solution)/shard_map/all_to_all | solution.py:578
  63.0 3.1 %copy-start.1 = (bf16[128,2048]{1,0:T(8,128)(2,1)S(1)}, bf16[128,2048]{1,0:T(8,128)(2,1)}, u32[]{:S(2)}) copy-start(bf16[128,2048]{1,0:T(8,128)(2,1)} %param.23) | copy-start | bytes 1572868
  63.0 3.1 %copy-start.3 = (f32[2048]{0:T(1024)S(1)}, f32[2048]{0:T(1024)}, u32[]{:S(2)}) copy-start(f32[2048]{0:T(1024)} %param.26) | copy-start | bytes 24580
  63.1 3.5 %copy-start.4 = (f32[2048]{0:T(1024)S(1)}, f32[2048]{0:T(1024)}, u32[]{:S(2)}) copy-start(f32[2048]{0:T(1024)} %param.27) | copy-start | bytes 24580
  66.1 57.2 %copy-start.7 = (bf16[1,2048,1024]{2,1,0:T(8,128)(2,1)S(1)}, bf16[1,2048,1024]{2,1,0:T(8,128)(2,1)}, u32[]{:S(2)}) copy-start(bf16[1,2048,1024]{2,1,0:T(8,128)(2,1)} %param.29) | copy-start | bytes 12582916
  122.1 1.3 copy-start
  136.3 46.6 %copy-start.5 = (f32[2048]{0:T(1024)S(1)}, f32[2048]{0:T(1024)}, u32[]{:S(2)}) copy-start(f32[2048]{0:T(1024)} %param.28) | copy-start | bytes 24580
